TPU v7x, 32 devices: a whole 2x2x4 slice. The times are simulated.
32 devices in a mesh: sp: 8 (over z, y), tp: 4 (over x, core).
Axes of the slice: x: 2, y: 2, z: 4, core: 2. Of those that a mesh axis runs over, the one named last changes fastest.
Arguments:
- query_nope: bfloat16 [1536, 4096], P('sp', 'tp'), may hold values from -6 to 6
- query_rope: bfloat16 [1536, 2048], P('sp', 'tp'), may hold values from -24 to 24
- latent: bfloat16 [1536, 512], P('sp'), may hold values from -6 to 6
- key_rope: bfloat16 [1536, 32], P('sp'), may hold values from -24 to 24
- latent_gain: float32 [512], replicated, may hold values from 0.1 to 1.9
- key_up: bfloat16 [512, 4096], P(None, 'tp'), may hold values from -0.25 to 0.25
- value_up: bfloat16 [512, 4096], P(None, 'tp'), may hold values from -0.25 to 0.25
- out_proj: bfloat16 [4096, 4096], P('tp'), may hold values from -0.09375 to 0.09375
- resid: bfloat16 [1536, 4096], P(('sp', 'tp')), may hold values from -6 to 6
- attn_gain: float32 [4096], replicated, may hold values from 0.1 to 1.9
- pre_gain: float32 [4096], replicated, may hold values from 0.1 to 1.9
- routes: int32 [1536, 2], P(('sp', 'tp')), may hold values from 0 to 7, all different within a row; in each aligned block of 48 rows (0 to 47, 48 to 95, ...) at most 24 rows name the same one
- route_weights: float32 [1536, 2], P(('sp', 'tp')), may hold values from 0.2 to 2
- expert_gate: bfloat16 [8, 4096, 1024], P('sp', None, 'tp'), may hold values from -0.09375 to 0.09375
- expert_up: bfloat16 [8, 4096, 1024], P('sp', None, 'tp'), may hold values from -0.09375 to 0.09375
- expert_down: bfloat16 [8, 1024, 4096], P('sp', 'tp'), may hold values from -0.1875 to 0.1875
- shared_gate: bfloat16 [4096, 1024], P(None, 'tp'), may hold values from -0.09375 to 0.09375
- shared_up: bfloat16 [4096, 1024], P(None, 'tp'), may hold values from -0.09375 to 0.09375
- shared_down: bfloat16 [1024, 4096], P('tp'), may hold values from -0.1875 to 0.1875
- moe_gain: float32 [4096], replicated, may hold values from 0.1 to 1.9
Outputs:
- output: bfloat16 [1536, 4096], P(('sp', 'tp'))
Inputs may be any that keep to these rules, and one draw needn't show every extreme that they name: `routes`: A row names 2 different experts. In each aligned block of 48 rows no expert is named by more than 24 rows, and in some block an expert is named by exactly 24 rows.
All inputs are finite; a program needn't handle non-finite values.
Results may differ from a plain program's by a relative error of at most 0.018.
Values may be sent and summed in bfloat16 or wider, within the bound.
A program may use at most 128 MiB of HBM per device.

v0:
```python
import math

import jax
import jax.numpy as jnp
from jax import lax
from jax.sharding import PartitionSpec as P

MODEL_DIM = 4096
NOPE_DIM = 64
ROPE_DIM = 32
VALUE_DIM = 64
TOP_K = 2


epsilon = 1e-06
theta_base = 10000.0


def rms_scale(values, gain_vector):
    return (
        values
        * lax.rsqrt(jnp.mean(values * values, axis=-1, keepdims=True) + epsilon)
        * gain_vector
    )


def rotate(values, positions):
    half_dim = values.shape[-1] // 2
    inverse = theta_base ** (-jnp.arange(half_dim, dtype=jnp.float32) / half_dim)
    angles = positions.astype(jnp.float32)[..., None] * inverse
    cosine = jnp.cos(angles)
    sine_part = jnp.sin(angles)
    first_half = values[..., :half_dim]
    second_half = values[..., half_dim:]
    return jnp.concatenate(
        [
            first_half * cosine - second_half * sine_part,
            second_half * cosine + first_half * sine_part,
        ],
        axis=-1,
    )


def expert_block(expert_in, gate_part, up_part, down_part):
    hidden = (
        jax.nn.silu(jnp.dot(expert_in, gate_part, preferred_element_type=jnp.float32))
        * jnp.dot(expert_in, up_part, preferred_element_type=jnp.float32)
    ).astype(jnp.bfloat16)
    return jnp.dot(hidden, down_part, preferred_element_type=jnp.float32).astype(jnp.bfloat16)


def dispatch_table(normed_rows, route_rows, experts, capacity):
    row_count = normed_rows.shape[0]
    flat_routes = route_rows.reshape(-1)
    onehot = (flat_routes[:, None] == jnp.arange(experts, dtype=jnp.int32)[None, :]).astype(
        jnp.int32
    )
    earlier = jnp.cumsum(onehot, axis=0) - onehot
    target = flat_routes * capacity + jnp.sum(earlier * onehot, axis=1)
    matches = (
        target.reshape(row_count, -1)[None, :, :]
        == jnp.arange(experts * capacity, dtype=jnp.int32)[:, None, None]
    )
    spread = jnp.any(matches, axis=2).astype(jnp.bfloat16)
    slot_table = jnp.dot(spread, normed_rows, preferred_element_type=jnp.float32).astype(
        jnp.bfloat16
    )
    return (slot_table.reshape(experts, capacity, normed_rows.shape[1]), target)


def on_device(
    query_nope,
    query_rope,
    latent,
    key_rope,
    latent_gain,
    key_up,
    value_up,
    out_proj,
    resid,
    attn_gain,
    pre_gain,
    routes,
    route_weights,
    expert_gate,
    expert_up,
    expert_down,
    shared_gate,
    shared_up,
    shared_down,
    moe_gain,
):
    local_rows = query_nope.shape[0]
    heads_here = query_nope.shape[1] // NOPE_DIM
    query_pos = lax.axis_index("sp") * local_rows + jnp.arange(local_rows, dtype=jnp.int32)
    last_query = lax.axis_index("sp") * local_rows + local_rows - 1
    query_rot = rotate(
        query_rope.astype(jnp.float32).reshape(local_rows, heads_here, ROPE_DIM), query_pos[:, None]
    ).astype(jnp.bfloat16)
    key_rot = rotate(key_rope.astype(jnp.float32), query_pos).astype(jnp.bfloat16)
    latent_normed = rms_scale(latent.astype(jnp.float32), latent_gain).astype(jnp.bfloat16)
    query_heads = query_nope.reshape(local_rows, heads_here, NOPE_DIM)
    score_scale = (NOPE_DIM + ROPE_DIM) ** (-0.5)

    def attend(state_now, latent_rows, rotary_rows, key_start):
        piece_rows = latent_rows.shape[0]
        keys_here = jnp.dot(latent_rows, key_up, preferred_element_type=jnp.float32).astype(
            jnp.bfloat16
        )
        keys_here = keys_here.reshape(piece_rows, heads_here, NOPE_DIM)
        values_here = jnp.dot(latent_rows, value_up, preferred_element_type=jnp.float32).astype(
            jnp.bfloat16
        )
        values_here = values_here.reshape(piece_rows, heads_here, VALUE_DIM)
        scores = (
            jnp.einsum("qhd,khd->hqk", query_heads, keys_here, preferred_element_type=jnp.float32)
            + jnp.einsum("qhr,kr->hqk", query_rot, rotary_rows, preferred_element_type=jnp.float32)
        ) * score_scale
        allowed = (key_start + jnp.arange(piece_rows, dtype=jnp.int32))[None, :] <= query_pos[
            :, None
        ]
        scores = jnp.where(allowed[None], scores, -1e30)
        running, total_sum, summed = state_now
        newest = jnp.maximum(running, jnp.max(scores, axis=-1))
        factor = jnp.exp(running - newest)
        exponent = jnp.exp(scores - newest[..., None])
        total_sum = total_sum * factor + jnp.sum(exponent, axis=-1)
        summed = summed * factor[..., None] + jnp.einsum(
            "hqk,khd->hqd",
            exponent.astype(jnp.bfloat16),
            values_here,
            preferred_element_type=jnp.float32,
        )
        return (newest, total_sum, summed)

    initial = (
        jnp.full((heads_here, local_rows), -1e30, jnp.float32),
        jnp.zeros((heads_here, local_rows), jnp.float32),
        jnp.zeros((heads_here, local_rows, VALUE_DIM), jnp.float32),
    )
    latent_piece = lax.all_gather(latent_normed, "sp", axis=0, tiled=True)
    rotary_piece = lax.all_gather(key_rot, "sp", axis=0, tiled=True)
    piece_rows = latent_piece.shape[0]
    step_rows = math.gcd(piece_rows, 512)

    def one_step(step_index, inner_state):
        offset = step_index * step_rows
        latent_rows = lax.dynamic_slice_in_dim(latent_piece, offset, step_rows, 0)
        rotary_rows = lax.dynamic_slice_in_dim(rotary_piece, offset, step_rows, 0)
        return lax.cond(
            offset <= last_query,
            lambda carried: attend(carried, latent_rows, rotary_rows, offset),
            lambda carried: carried,
            inner_state,
        )

    running, total_sum, summed = lax.fori_loop(0, piece_rows // step_rows, one_step, initial)
    attention = (
        (summed / total_sum[..., None])
        .transpose(1, 0, 2)
        .reshape(local_rows, heads_here * VALUE_DIM)
    )
    attention = attention.astype(jnp.bfloat16)
    projected = lax.psum_scatter(
        jnp.dot(attention, out_proj, preferred_element_type=jnp.float32).astype(jnp.bfloat16),
        "tp",
        scatter_dimension=0,
        tiled=True,
    ).astype(jnp.float32)
    mixed = (resid.astype(jnp.float32) + rms_scale(projected, attn_gain)).astype(jnp.bfloat16)
    normed = rms_scale(mixed.astype(jnp.float32), pre_gain).astype(jnp.bfloat16)
    rows_here = resid.shape[0]
    tp_count = lax.axis_size("tp")
    experts = lax.axis_size("sp")
    capacity = max(2, 2 * rows_here * TOP_K // experts)
    own_table, target = dispatch_table(normed, routes, experts, capacity)
    arrived = lax.all_to_all(own_table, "sp", split_axis=0, concat_axis=0, tiled=True)
    column = lax.all_gather(arrived[None], "tp", axis=0, tiled=True)
    group_normed = lax.all_gather(normed, "tp", axis=0, tiled=True)
    expert_out = expert_block(
        column.reshape(-1, MODEL_DIM), expert_gate[0], expert_up[0], expert_down[0]
    )
    shared_part = expert_block(group_normed, shared_gate, shared_up, shared_down)
    routed_sum, shared_sum = (
        lax.psum_scatter(
            expert_out.reshape(column.shape).astype(jnp.float32).astype(jnp.bfloat16),
            "tp",
            scatter_dimension=0,
            tiled=True,
        ).astype(jnp.float32),
        lax.psum_scatter(
            shared_part.reshape(tp_count, rows_here, MODEL_DIM)
            .astype(jnp.float32)
            .astype(jnp.bfloat16),
            "tp",
            scatter_dimension=0,
            tiled=True,
        ).astype(jnp.float32),
    )
    expert_rows = lax.all_to_all(
        routed_sum.astype(jnp.bfloat16), "sp", split_axis=1, concat_axis=1, tiled=True
    ).reshape(-1, MODEL_DIM)
    shared_out = shared_sum.reshape(rows_here, MODEL_DIM)
    picked = expert_rows[target].astype(jnp.float32).reshape(rows_here, TOP_K, MODEL_DIM)
    routed = jnp.sum(picked * route_weights[..., None], axis=1)
    moe = shared_out + routed
    return (mixed.astype(jnp.float32) + rms_scale(moe, moe_gain)).astype(jnp.bfloat16)


def solution(mesh):
    in_specs = (
        P("sp", "tp"),
        P("sp", "tp"),
        P("sp", None),
        P("sp", None),
        P(),
        P(None, "tp"),
        P(None, "tp"),
        P("tp", None),
        P(("sp", "tp"), None),
        P(),
        P(),
        P(("sp", "tp"), None),
        P(("sp", "tp"), None),
        P("sp", None, "tp"),
        P("sp", None, "tp"),
        P("sp", "tp", None),
        P(None, "tp"),
        P(None, "tp"),
        P("tp", None),
        P(),
    )
    out_specs = P(("sp", "tp"), None)
    return jax.shard_map(
        on_device, mesh=mesh, in_specs=in_specs, out_specs=out_specs, check_vma=False
    )
```

profile of v0, /device:TPU:0, one launch (start us, length us, event | category | flops | bytes accessed | tf_op | source)
XLA Modules:
  0.0 459.1 jit_solution(2781892771527778260)
XLA Ops:
  11.5 32.8 %all-gather.1 = bf16[8,192,32]{1,2,0:T(8,128)(2,1)S(1)} all-gather(bf16[1,192,32]{1,2,0:T(8,128)(2,1)S(1)} %maximum_bitcast_fusion), channel_id=1, replica_groups=mesh['sp'=8,'tp'=4] {'sp'}, dimensions={0}, use_global_device_ids=true | all-gather | bytes 110592 | tf_op jit(solution)/shard_map/all_gather | solution.py:142
  46.3 10.5 %all-gather.6.cloned.1.call-done = bf16[1536,512]{1,0:T(8,128)(2,1)} async-done(((bf16[192,512]{1,0:T(8,128)(2,1)}), bf16[1536,512]{1,0:T(8,128)(2,1)}) %all-gather.6.cloned.1.call-update) | async-done | bytes 1572880 | tf_op jit(solution)/shard_map/all_gather | solution.py:141
  58.0 22.1 %while.18 = (s32[]{:T(128)}, f32[16,192]{1,0:T(8,128)S(1)}, f32[16,192]{1,0:T(8,128)S(1)}, f32[16,192,64]{1,2,0:T(8,128)}, s32[]{:T(128)}, /*index=5*/bf16[1536,...) while((s32[]{:T(128)}, f32[16,192]{1,0:T(8,128)S(1)}, ...), condition=%wide.region_6.7_spmd.clone, body=%wide.region_1.6_spmd.clone.sunk | while | flops 1591188224 | bytes 74948008 | solution.py:157
  58.0 22.1 %conditional.3 = ((f32[16,192]{1,0:T(8,128)S(1)}, f32[16,192]{1,0:T(8,128)S(1)}, f32[16,192,64]{1,2,0:T(8,128)})) conditional(s32[]{:T(128)} %convert_element_type.198, (f32[16,192]{1,0:T(8,128)S(1)}, f32[16,192]{1,0:T(8,128)S(1)}, f32[16,192,64]{1,2,0:T(8,128)}) %tuple.60, (s32[]{:T(128)}, s32[]{:T(128)}, bf16[1536,512]{1,0:T(8,128)(2,1)}, ...), branch_computations={%region_2.0_spmd, %region_3.5_spmd} | conditional | flops 1591188224 | bytes 74946960 | solution.py:150
  58.0 3.1 convolution_convert_fusion.1
  64.8 2.9 fusion.63
  70.3 2.8 convolution_convert_fusion
  74.6 5.4 %fusion.9 = f32[16,192,64]{1,2,0:T(8,128)} fusion(bf16[512,16,64]{0,2,1:T(8,128)(2,1)S(1)} %bitcast.74, f32[16,192,512]{2,1,0:T(8,128)} %copy-done.1, f32[16,192]{1,0:T(8,128)S(1)} %max.5, f32[16,192,64]{1,2,0:T(8,128)} %get-tuple-element.325, f32[16,192]{1,0:T(8,128)S(1)} %get-tuple-element.405), kind=kOutput, calls=%fused_computation.12 | convolution fusion | flops 204865536 | bytes 8937472 | tf_op jit(solution)/shard_map/while/body/eval_jaxpr/cond/branch_1_fun/hqk,khd->hqd/dot_general | solution.py:128
  81.4 6.4 %convolution_convert_fusion.5 = bf16[192,4096]{1,0:T(8,128)(2,1)} fusion(bf16[192,1024]{0,1:T(8,128)(2,1)S(1)} %bitcast.80, bf16[1024,4096]{1,0:T(8,128)(2,1)} %param.31), kind=kOutput, calls=%fused_computation.28 | convolution fusion | flops 1611399168 | bytes 10354688 | tf_op jit(solution)/shard_map/dot_general | solution.py:165
  88.9 69.8 %reduce-scatter.4.cloned.1.call-done = bf16[48,4096]{1,0:T(8,128)(2,1)} async-done(((bf16[192,4096]{1,0:T(8,128)(2,1)}), bf16[48,4096]{1,0:T(8,128)(2,1)}) %reduce-scatter.4.cloned.1.call-update) | async-done | bytes 393232 | tf_op jit(solution)/shard_map/reduce_scatter | solution.py:164
  162.0 42.3 %all_to_all.10 = bf16[8,24,4096]{2,1,0:T(8,128)(2,1)} all-to-all(bf16[8,24,4096]{2,1,0:T(8,128)(2,1)S(1)} %bitcast.79), channel_id=1, replica_groups=mesh['sp'=8,'tp'=4] {'sp'}, dimensions={0} | all-to-all | bytes 3145728 | tf_op jit(solution)/shard_map/all_to_all | solution.py:177
  205.1 43.8 %all-gather.10.cloned.1.call-done = bf16[32,24,4096]{2,1,0:T(8,128)(2,1)} async-done(((bf16[8,24,4096]{2,1,0:T(8,128)(2,1)}), bf16[32,24,4096]{2,1,0:T(8,128)(2,1)}) %all-gather.10.cloned.1.call-update) | async-done | bytes 6291472 | tf_op jit(solution)/shard_map/all_gather | solution.py:178
  248.9 6.1 %fusion.22 = f32[768,256]{1,0:T(8,128)} fusion(bf16[768,4096]{1,0:T(8,128)(2,1)} %bitcast.82, bf16[1,4096,256]{2,1,0:T(8,128)(2,1)} %param.37), kind=kOutput, calls=%fused_computation.32 | convolution fusion | flops 1610612736 | bytes 9175040 | tf_op jit(solution)/shard_map/dot_general | solution.py:46
  255.0 13.3 %convolution_convert_fusion.2 = bf16[768,4096]{1,0:T(8,128)(2,1)} fusion(bf16[1,256,4096]{2,1,0:T(8,128)(2,1)S(1)} %copy-done, bf16[768,4096]{1,0:T(8,128)(2,1)} %bitcast.83, bf16[1,4096,256]{2,1,0:T(8,128)(2,1)} %param.38, f32[768,256]{1,0:T(8,128)} %fusion.22), kind=kOutput, calls=%fused_computation.25 | convolution fusion | flops 3225550848 | bytes 17563648 | tf_op jit(solution)/shard_map/dot_general | solution.py:49
  268.2 6.3 %copy.71 = bf16[4,8,24,4096]{3,2,0,1:T(8,128)(2,1)} copy(bf16[4,8,24,4096]{3,2,1,0:T(8,128)(2,1)} %bitcast.77) | data formatting | bytes 12582912 | tf_op jit(solution)/shard_map/reshape | solution.py:186
  275.8 2.6 fusion.65
  278.4 6.9 %convolution_convert_fusion.4 = bf16[192,4096]{1,0:T(8,128)(2,1)} fusion(bf16[256,4096]{1,0:T(8,128)(2,1)} %param.42, bf16[192,4096]{1,0:T(8,128)(2,1)} %all-gather.8.cloned.1.call-done, bf16[4096,256]{1,0:T(8,128)(2,1)} %param.41, f32[192,256]{1,0:T(8,128)S(1)} %fusion.65), kind=kOutput, calls=%fused_computation.27 | convolution fusion | flops 806387712 | bytes 7536640 | tf_op jit(solution)/shard_map/dot_general | solution.py:49
  285.3 108.8 %all-reduce.3.cloned.1.call-done = bf16[4,8,24,4096]{3,2,0,1:T(8,128)(2,1)} async-done(((bf16[4,8,24,4096]{3,2,0,1:T(8,128)(2,1)}), bf16[4,8,24,4096]{3,2,0,1:T(8,128)(2,1)}) %all-reduce.3.cloned.1.call-update) | async-done | bytes 6291472
  394.2 3.3 constant_dynamic-slice_fusion
  397.5 5.6 %all-to-all-start.1 = ((bf16[1,8,24,4096]{3,2,0,1:T(8,128)(2,1)}), bf16[1,8,24,4096]{3,2,0,1:T(8,128)(2,1)}, u32[]{:S(2)}, u32[]{:S(2)}) async-start(bf16[1,8,24,4096]{3,2,0,1:T(8,128)(2,1)} %constant_dynamic-slice_fusion), calls=%async_computation.3 | async-start | bytes 3145728 | tf_op jit(solution)/shard_map/all_to_all | solution.py:200
  403.4 36.5 %all-to-all-done.1 = bf16[1,8,24,4096]{3,2,0,1:T(8,128)(2,1)} async-done(((bf16[1,8,24,4096]{3,2,0,1:T(8,128)(2,1)}), bf16[1,8,24,4096]{3,2,0,1:T(8,128)(2,1)}, u32[]{:S(2)}, u32[]{:S(2)}) %all-to-all-start.1) | async-done | bytes 1572896 | tf_op jit(solution)/shard_map/all_to_all | solution.py:200
  439.8 3.4 gather_fusion
  443.2 2.1 reshape.251
  445.4 3.6 multiply_reduce_fusion
  (94 shorter events, 27.0 us)
Async XLA Ops:
  6.5 248.4 %copy-start = (bf16[1,256,4096]{2,1,0:T(8,128)(2,1)S(1)}, bf16[1,256,4096]{2,1,0:T(8,128)(2,1)}, u32[]{:S(2)}) copy-start(bf16[1,256,4096]{2,1,0:T(8,128)(2,1)} %param.39) | copy-start | bytes 6291460
  6.5 38.6 %copy-start.3 = (bf16[192,1024]{1,0:T(8,128)(2,1)S(1)}, bf16[192,1024]{1,0:T(8,128)(2,1)}, u32[]{:S(2)}) copy-start(bf16[192,1024]{1,0:T(8,128)(2,1)} %param.24) | copy-start | bytes 1179652
  6.5 50.3 %all-gather.6.cloned.1.call-start = ((), (), s32[]{:S(2)}) async-start(), calls=%async_computation.4 | async-start | bytes 1769472 | tf_op jit(solution)/shard_map/all_gather | solution.py:141
  9.5 149.1 %reduce-scatter.4.cloned.1.call-start = ((), (), s32[]{:S(2)}) async-start(), calls=%async_computation.5 | async-start | bytes 1966080 | tf_op jit(solution)/shard_map/reduce_scatter | solution.py:164
  67.7 2.6 copy-start.1
  67.7 2.6 copy-start.10
  81.4 6.5 %copy-start.8 = (s32[48,2]{0,1:T(2,128)S(1)}, s32[48,2]{0,1:T(2,128)}, u32[]{:S(2)}) copy-start(s32[48,2]{0,1:T(2,128)} %param.35) | copy-start | bytes 1156
  87.8 72.0 %copy-start.4 = (bf16[48,4096]{1,0:T(8,128)(2,1)S(1)}, bf16[48,4096]{1,0:T(8,128)(2,1)}, u32[]{:S(2)}) copy-start(bf16[48,4096]{1,0:T(8,128)(2,1)} %param.32) | copy-start | bytes 1179652
  87.8 72.0 %copy-start.5 = (f32[4096]{0:T(1024)S(1)}, f32[4096]{0:T(1024)}, u32[]{:S(2)}) copy-start(f32[4096]{0:T(1024)} %param.33) | copy-start | bytes 49156
  87.8 73.4 %copy-start.7 = (f32[4096]{0:T(1024)S(1)}, f32[4096]{0:T(1024)}, u32[]{:S(2)}) copy-start(f32[4096]{0:T(1024)} %param.34) | copy-start | bytes 49156
  87.9 161.0 %all-gather.10.cloned.1.call-start = ((), (), s32[]{:S(2)}) async-start(), calls=%async_computation.8 | async-start | bytes 7864320 | tf_op jit(solution)/shard_map/all_gather | solution.py:178
  161.4 42.9 %copy-start.2 = (bf16[48,4096]{1,0:T(8,128)(2,1)}, bf16[48,4096]{1,0:T(8,128)(2,1)S(1)}, u32[]{:S(2)}) copy-start(bf16[48,4096]{1,0:T(8,128)(2,1)S(1)} %fusion.39) | copy-start | bytes 1179652
  204.3 71.5 %all-gather.8.cloned.1.call-start = ((), (), s32[]{:S(2)}) async-start(), calls=%async_computation.6 | async-start | bytes 1966080 | tf_op jit(solution)/shard_map/all_gather | solution.py:179
  204.9 189.3 %all-reduce.3.cloned.1.call-start = ((), (), s32[]{:S(2)}) async-start(), calls=%async_computation.9 | async-start | bytes 12582912
  274.5 0.7 copy-start.11
  274.5 174.5 %reduce-scatter.6.cloned.1.call-start = ((), (), s32[]{:S(2)}) async-start(), calls=%async_computation.7 | async-start | bytes 1966080 | tf_op jit(solution)/shard_map/reduce_scatter | solution.py:191
  397.5 5.8 %copy-start.9 = (f32[48,2]{0,1:T(2,128)S(1)}, f32[48,2]{0,1:T(2,128)}, u32[]{:S(2)}) copy-start(f32[48,2]{0,1:T(2,128)} %param.36) | copy-start | bytes 1156
  397.5 42.4 %all-to-all-start.1 = ((bf16[1,8,24,4096]{3,2,0,1:T(8,128)(2,1)}), bf16[1,8,24,4096]{3,2,0,1:T(8,128)(2,1)}, u32[]{:S(2)}, u32[]{:S(2)}) async-start(bf16[1,8,24,4096]{3,2,0,1:T(8,128)(2,1)} %constant_dynamic-slice_fusion), calls=%async_computation.3 | async-start | bytes 3145728 | tf_op jit(solution)/shard_map/all_to_all | solution.py:200
  445.4 4.9 %copy-start.6 = (f32[4096]{0:T(1024)S(1)}, f32[4096]{0:T(1024)}, u32[]{:S(2)}) copy-start(f32[4096]{0:T(1024)} %param.43) | copy-start | bytes 49156
Sparse Core Ops, SparseCore 0:
  9.6 47.1 all-gather.5
  88.0 70.5 reduce-scatter.3
  204.4 44.4 all-gather.9
  250.3 19.6 all-gather.7
  274.6 119.4 all-reduce.2
  396.5 28.2 reduce-scatter.5
where the time goes:
time: 460 us; the launch traced here: 459 us
  waiting for transfers between devices  270 us (59%)
  blocking collectives  75 us (16%)
  matrix products  52.1 us (11%)
  local copies, waits for them, and re-layouts  25 us (5%)
  other arithmetic  17.1 us (4%)
  between operations  13.7 us (3%)
  starting transfers between devices  6.04 us (1%)
    unnamed x7, waiting for transfers between devices  109 us
    reduce_scatter x1, waiting for transfers between devices, on_device(): lax.psum_scatter(jnp.dot(attention, out_proj, preferred_element_type=jnp....  69.8 us
    all_gather x1, waiting for transfers between devices, on_device(): column = lax.all_gather(arrived[None], 'tp', axis=0, tiled=True)  43.8 us
    all_to_all x1, blocking collectives, on_device(): lax.all_to_all(own_table, 'sp', split_axis=0, concat_axis=0, tiled=True)  42.3 us
    all_to_all x1, waiting for transfers between devices, on_device(): lax.all_to_all(routed_sum.astype(jnp.bfloat16), 'sp', split_axis=1, conca...  36.5 us
    all_gather x1, blocking collectives, on_device(): rotary_piece = lax.all_gather(key_rot, 'sp', axis=0, tiled=True)  32.8 us
    dot_general x2, matrix products, expert_block(): jnp.dot(hidden, down_part, preferred_element_type=jnp.float32)  20.1 us
    all_gather x1, waiting for transfers between devices, on_device(): latent_piece = lax.all_gather(latent_normed, 'sp', axis=0, tiled=True)  10.5 us
  transfers between devices with their start and end apart: 7, of which 5 were waited for; matrix products, arithmetic and copies ran while one was open for 12% of the time, Pallas kernels for 0%

commit v1 on v0

--- a/solution.py
+++ b/solution.py
@@ -1,8 +1,11 @@
+import functools
 import math
 
 import jax
 import jax.numpy as jnp
 from jax import lax
+from jax.experimental import pallas as pl
+from jax.experimental.pallas import tpu as pltpu
 from jax.sharding import PartitionSpec as P
 
 MODEL_DIM = 4096
@@ -49,7 +52,336 @@
     return jnp.dot(hidden, down_part, preferred_element_type=jnp.float32).astype(jnp.bfloat16)
 
 
-def dispatch_table(normed_rows, route_rows, experts, capacity):
+def remote_copy(source, dest, send_sem, recv_sem, sp_index, tp_index):
+    return pltpu.make_async_remote_copy(
+        src_ref=source,
+        dst_ref=dest,
+        send_sem=send_sem,
+        recv_sem=recv_sem,
+        device_id=(sp_index, tp_index),
+        device_id_type=pl.DeviceIdType.MESH,
+    )
+
+
+def enter(me, tp_me, sp_count):
+    barrier = pltpu.get_barrier_semaphore()
+    for bit in (1, 2):
+        pl.semaphore_signal(
+            barrier,
+            inc=1,
+            device_id=(me, flip(tp_me, bit)),
+            device_id_type=pl.DeviceIdType.MESH,
+        )
+
+    def greet(k, carry):
+        pl.semaphore_signal(
+            barrier,
+            inc=1,
+            device_id=(lax.rem(me + 1 + k, sp_count), tp_me),
+            device_id_type=pl.DeviceIdType.MESH,
+        )
+        return carry
+
+    lax.fori_loop(0, sp_count - 1, greet, 0)
+    pl.semaphore_wait(barrier, sp_count + 1)
+
+
+def flip(tp_me, bit):
+    high, low = tp_me // 2, lax.rem(tp_me, 2)
+    return high * 2 + (1 - low) if bit == 1 else (1 - high) * 2 + low
+
+
+def add(*parts):
+    total = parts[0].astype(jnp.float32)
+    for part in parts[1:]:
+        total = total + part.astype(jnp.float32)
+    return total
+
+
+class PairSum:
+    def __init__(self, parts, got1, half, got2, sems, me, tp_me):
+        self.parts, self.got1, self.half, self.got2 = parts, got1, half, got2
+        self.sems, self.me, self.tp_me = sems, me, tp_me
+        self.high, self.low = tp_me // 2, lax.rem(tp_me, 2)
+
+    def first(self, side, e):
+        return remote_copy(
+            self.parts.at[side, 1 - self.low, e],
+            self.got1.at[side, e],
+            self.sems.at[0, side, e],
+            self.sems.at[1, side, e],
+            self.me,
+            flip(self.tp_me, 1),
+        )
+
+    def second(self, e):
+        return remote_copy(
+            self.half.at[e],
+            self.got2.at[e],
+            self.sems.at[0, 2, e],
+            self.sems.at[1, 2, e],
+            self.me,
+            flip(self.tp_me, 2),
+        )
+
+    def start(self, e):
+        for side in range(2):
+            self.first(side, e).start()
+
+    def middle(self, e):
+        for side in range(2):
+            self.first(side, e).wait_recv()
+        other = 1 - self.high
+        self.half[e] = add(self.parts[other, self.low, e], self.got1[other, e]).astype(
+            self.half.dtype
+        )
+        self.second(e).start()
+
+    def finish(self, e):
+        self.second(e).wait_recv()
+        return add(
+            self.parts[self.high, self.low, e], self.got1[self.high, e], self.got2[e]
+        )
+
+    def drain(self, e):
+        for side in range(2):
+            self.first(side, e).wait_send()
+        self.second(e).wait_send()
+
+
+def loop(count, body):
+    def step(k, carry):
+        body(k)
+        return carry
+
+    lax.fori_loop(0, count, step, 0)
+
+
+def reduce_kernel(parts, out, got1, half, got2, sems):
+    me, tp_me = lax.axis_index("sp"), lax.axis_index("tp")
+    enter(me, tp_me, 1)
+    pair = PairSum(parts, got1, half, got2, sems, me, tp_me)
+    pieces = parts.shape[2]
+    loop(pieces, pair.start)
+    loop(pieces, pair.middle)
+
+    def close(e):
+        out[e] = pair.finish(e)
+
+    loop(pieces, close)
+    loop(pieces, pair.drain)
+
+
+def pair_scratch(shape):
+    pieces, block = shape[2], tuple(shape[2:])
+    return [
+        pltpu.VMEM((2,) + block, jnp.bfloat16),
+        pltpu.VMEM(block, jnp.bfloat16),
+        pltpu.VMEM(block, jnp.bfloat16),
+        pltpu.SemaphoreType.DMA((2, 3, pieces)),
+    ]
+
+
+IN_VMEM = pl.BlockSpec(memory_space=pltpu.VMEM)
+
+
+def comm_params(number):
+    return pltpu.CompilerParams(
+        collective_id=number, has_side_effects=True, vmem_limit_bytes=60 * 1024 * 1024
+    )
+
+
+def tp_reduce(parts):
+    return pl.pallas_call(
+        reduce_kernel,
+        out_shape=jax.ShapeDtypeStruct(parts.shape[2:], jnp.float32),
+        in_specs=[IN_VMEM],
+        out_specs=IN_VMEM,
+        scratch_shapes=pair_scratch(parts.shape),
+        compiler_params=comm_params(0),
+    )(parts)
+
+
+def dispatch_kernel(sp_count, table, normed, column, group, to_sp, to_low, to_high, relay, norm_sems):
+    me, tp_me = lax.axis_index("sp"), lax.axis_index("tp")
+    low_peer, high_peer = flip(tp_me, 1), flip(tp_me, 2)
+    last = sp_count - 1
+    enter(me, tp_me, sp_count)
+
+    def source_of(k):
+        return lax.rem(me + 2 * sp_count - 1 - k, sp_count)
+
+    def norm_copy(index, source, slot, peer):
+        return remote_copy(
+            source, group.at[slot], norm_sems.at[0, index], norm_sems.at[1, index], me, peer
+        )
+
+    norm_low = norm_copy(0, normed, tp_me, low_peer)
+    norm_high = norm_copy(1, normed, tp_me, high_peer)
+    norm_relay = norm_copy(2, group.at[high_peer], high_peer, low_peer)
+    norm_low.start()
+    norm_high.start()
+
+    def spread(k):
+        e = lax.rem(me + 1 + k, sp_count)
+        return remote_copy(
+            table.at[e], column.at[tp_me, me], to_sp.at[0, k], to_sp.at[1, k], e, tp_me
+        )
+
+    def forward(sems, k, source, slot, peer):
+        return remote_copy(
+            source, column.at[slot, source_of(k)], sems.at[0, k], sems.at[1, k], me, peer
+        )
+
+    def own_low():
+        return forward(to_low, last, table.at[me], tp_me, low_peer)
+
+    def own_high():
+        return forward(to_high, last, table.at[me], tp_me, high_peer)
+
+    def low(k):
+        return forward(to_low, k, column.at[tp_me, source_of(k)], tp_me, low_peer)
+
+    def high(k):
+        return forward(to_high, k, column.at[tp_me, source_of(k)], tp_me, high_peer)
+
+    def relayed(k):
+        return forward(relay, k, column.at[high_peer, source_of(k)], high_peer, low_peer)
+
+    own_high().start()
+    own_low().start()
+    loop(last, lambda k: spread(k).start())
+    group[tp_me] = normed[...]
+    column[tp_me, me] = table[me]
+    norm_high.wait_recv()
+    norm_relay.start()
+
+    def arrive(k):
+        spread(k).wait_recv()
+        high(k).start()
+        low(k).start()
+
+    loop(last, arrive)
+
+    def pass_on(k):
+        high(k).wait_recv()
+        relayed(k).start()
+
+    pass_on(last)
+    loop(last, pass_on)
+
+    def settle(k):
+        low(k).wait_recv()
+        relayed(k).wait_recv()
+        relayed(k).wait_send()
+
+    loop(sp_count, settle)
+
+    def sent(k):
+        spread(k).wait_send()
+        low(k).wait_send()
+        high(k).wait_send()
+
+    loop(last, sent)
+    own_low().wait_send()
+    own_high().wait_send()
+    norm_low.wait()
+    norm_high.wait_send()
+    norm_relay.wait()
+
+
+def dispatch(table, normed):
+    sp_count, tp_count = lax.axis_size("sp"), lax.axis_size("tp")
+    ring = pltpu.SemaphoreType.DMA((2, sp_count))
+    return pl.pallas_call(
+        functools.partial(dispatch_kernel, sp_count),
+        out_shape=(
+            jax.ShapeDtypeStruct((tp_count,) + table.shape, table.dtype),
+            jax.ShapeDtypeStruct((tp_count,) + normed.shape, normed.dtype),
+        ),
+        in_specs=[IN_VMEM] * 2,
+        out_specs=(IN_VMEM, IN_VMEM),
+        scratch_shapes=[ring, ring, ring, ring, pltpu.SemaphoreType.DMA((2, 3))],
+        compiler_params=comm_params(1),
+    )(table, normed)
+
+
+def return_kernel(
+    sp_count,
+    parts,
+    shared,
+    rows_out,
+    shared_out,
+    got1,
+    half,
+    got2,
+    sems,
+    shared_got1,
+    shared_half,
+    shared_got2,
+    shared_sems,
+    final,
+    back,
+):
+    me, tp_me = lax.axis_index("sp"), lax.axis_index("tp")
+    last = sp_count - 1
+    enter(me, tp_me, sp_count)
+    routed = PairSum(parts, got1, half, got2, sems, me, tp_me)
+    common = PairSum(shared, shared_got1, shared_half, shared_got2, shared_sems, me, tp_me)
+    common_pieces = shared.shape[2]
+
+    def owner(k):
+        return lax.rem(me + 1 + k, sp_count)
+
+    def home(k):
+        e = owner(k)
+        return remote_copy(
+            final.at[e], rows_out.at[me], back.at[0, k], back.at[1, k], e, tp_me
+        )
+
+    loop(sp_count, lambda k: routed.start(owner(k)))
+    loop(common_pieces, common.start)
+    loop(sp_count, lambda k: routed.middle(owner(k)))
+    loop(common_pieces, common.middle)
+
+    def deliver(k):
+        e = owner(k)
+        final[e] = routed.finish(e).astype(final.dtype)
+        home(k).start()
+
+    loop(last, deliver)
+    rows_out[me] = routed.finish(me).astype(rows_out.dtype)
+
+    def close(e):
+        shared_out[e] = common.finish(e)
+
+    loop(common_pieces, close)
+    loop(sp_count, routed.drain)
+    loop(common_pieces, common.drain)
+    loop(last, lambda k: home(k).wait())
+
+
+def give_back(parts, shared):
+    sp_count = lax.axis_size("sp")
+    return pl.pallas_call(
+        functools.partial(return_kernel, sp_count),
+        out_shape=(
+            jax.ShapeDtypeStruct(parts.shape[2:], parts.dtype),
+            jax.ShapeDtypeStruct(shared.shape[2:], jnp.float32),
+        ),
+        in_specs=[IN_VMEM] * 2,
+        out_specs=(IN_VMEM, IN_VMEM),
+        scratch_shapes=pair_scratch(parts.shape)
+        + pair_scratch(shared.shape)
+        + [
+            pltpu.VMEM(parts.shape[2:], parts.dtype),
+            pltpu.SemaphoreType.DMA((2, sp_count)),
+        ],
+        compiler_params=comm_params(2),
+    )(parts, shared)
+
+
+def dispatch_table(normed_rows, route_rows, route_weights, experts, capacity):
     row_count = normed_rows.shape[0]
     flat_routes = route_rows.reshape(-1)
     onehot = (flat_routes[:, None] == jnp.arange(experts, dtype=jnp.int32)[None, :]).astype(
@@ -65,7 +397,8 @@
     slot_table = jnp.dot(spread, normed_rows, preferred_element_type=jnp.float32).astype(
         jnp.bfloat16
     )
-    return (slot_table.reshape(experts, capacity, normed_rows.shape[1]), target)
+    combine = jnp.sum(jnp.where(matches, route_weights[None], 0.0), axis=2).T
+    return (slot_table.reshape(experts, capacity, normed_rows.shape[1]), combine)
 
 
 def on_device(
@@ -138,8 +471,11 @@
         jnp.zeros((heads_here, local_rows), jnp.float32),
         jnp.zeros((heads_here, local_rows, VALUE_DIM), jnp.float32),
     )
-    latent_piece = lax.all_gather(latent_normed, "sp", axis=0, tiled=True)
-    rotary_piece = lax.all_gather(key_rot, "sp", axis=0, tiled=True)
+    gathered = lax.all_gather(
+        jnp.concatenate([latent_normed, key_rot], axis=1), "sp", axis=0, tiled=True
+    )
+    latent_piece = gathered[:, : latent.shape[1]]
+    rotary_piece = gathered[:, latent.shape[1] :]
     piece_rows = latent_piece.shape[0]
     step_rows = math.gcd(piece_rows, 512)
 
@@ -161,48 +497,38 @@
         .reshape(local_rows, heads_here * VALUE_DIM)
     )
     attention = attention.astype(jnp.bfloat16)
-    projected = lax.psum_scatter(
-        jnp.dot(attention, out_proj, preferred_element_type=jnp.float32).astype(jnp.bfloat16),
-        "tp",
-        scatter_dimension=0,
-        tiled=True,
-    ).astype(jnp.float32)
+    rows_here = resid.shape[0]
+    model_dim = resid.shape[1]
+    piece = math.gcd(rows_here, 16)
+    projected = tp_reduce(
+        jnp.dot(attention, out_proj, preferred_element_type=jnp.float32)
+        .astype(jnp.bfloat16)
+        .reshape(2, 2, -1, piece, model_dim)
+    ).reshape(rows_here, model_dim)
     mixed = (resid.astype(jnp.float32) + rms_scale(projected, attn_gain)).astype(jnp.bfloat16)
     normed = rms_scale(mixed.astype(jnp.float32), pre_gain).astype(jnp.bfloat16)
-    rows_here = resid.shape[0]
-    tp_count = lax.axis_size("tp")
     experts = lax.axis_size("sp")
     capacity = max(2, 2 * rows_here * TOP_K // experts)
-    own_table, target = dispatch_table(normed, routes, experts, capacity)
-    arrived = lax.all_to_all(own_table, "sp", split_axis=0, concat_axis=0, tiled=True)
-    column = lax.all_gather(arrived[None], "tp", axis=0, tiled=True)
-    group_normed = lax.all_gather(normed, "tp", axis=0, tiled=True)
+    own_table, combine = dispatch_table(normed, routes, route_weights, experts, capacity)
+    column, group_normed = dispatch(own_table, normed)
     expert_out = expert_block(
-        column.reshape(-1, MODEL_DIM), expert_gate[0], expert_up[0], expert_down[0]
-    )
-    shared_part = expert_block(group_normed, shared_gate, shared_up, shared_down)
-    routed_sum, shared_sum = (
-        lax.psum_scatter(
-            expert_out.reshape(column.shape).astype(jnp.float32).astype(jnp.bfloat16),
-            "tp",
-            scatter_dimension=0,
-            tiled=True,
-        ).astype(jnp.float32),
-        lax.psum_scatter(
-            shared_part.reshape(tp_count, rows_here, MODEL_DIM)
-            .astype(jnp.float32)
-            .astype(jnp.bfloat16),
-            "tp",
-            scatter_dimension=0,
-            tiled=True,
-        ).astype(jnp.float32),
-    )
-    expert_rows = lax.all_to_all(
-        routed_sum.astype(jnp.bfloat16), "sp", split_axis=1, concat_axis=1, tiled=True
-    ).reshape(-1, MODEL_DIM)
-    shared_out = shared_sum.reshape(rows_here, MODEL_DIM)
-    picked = expert_rows[target].astype(jnp.float32).reshape(rows_here, TOP_K, MODEL_DIM)
-    routed = jnp.sum(picked * route_weights[..., None], axis=1)
+        column.reshape(-1, model_dim), expert_gate[0], expert_up[0], expert_down[0]
+    )
+    shared_part = expert_block(
+        group_normed.reshape(-1, model_dim), shared_gate, shared_up, shared_down
+    )
+    expert_rows, shared_sum = give_back(
+        expert_out.reshape(2, 2, experts, capacity, model_dim),
+        shared_part.reshape(2, 2, -1, piece, model_dim),
+    )
+    expert_rows = expert_rows.reshape(-1, model_dim)
+    shared_out = shared_sum.reshape(rows_here, model_dim)
+    upper = combine.astype(jnp.bfloat16)
+    lower = (combine - upper.astype(jnp.float32)).astype(jnp.bfloat16)
+    both = jnp.dot(
+        jnp.concatenate([upper, lower], axis=0), expert_rows, preferred_element_type=jnp.float32
+    )
+    routed = both[:rows_here] + both[rows_here:]
     moe = shared_out + routed
     return (mixed.astype(jnp.float32) + rms_scale(moe, moe_gain)).astype(jnp.bfloat16)
 

time: 460 us -> 314 us (0.68)
  waiting for transfers between devices: 270 us -> 47.4 us
  Pallas kernels: 0 us -> 175 us
  blocking collectives: 75 us -> 0 us
  local copies, waits for them, and re-layouts: 25 us -> 12.5 us
  starting transfers between devices: 6.04 us -> 0.03 us
  other arithmetic: 17.1 us -> 11.9 us
    pallas_call x0 -> x3, Pallas kernels: none -> 175 us  [the longest x1 98.6 us: dispatch(): pl.pallas_call(functools.partial(dispatch_kernel, sp_count), out_shape=(j...]
    unnamed x7 -> x1, waiting for transfers between devices: 109 us -> 0.02 us
    reduce_scatter x2 -> x0, waiting for transfers between devices: 69.8 us -> none  [the longest x1 69.8 us: on_device(): lax.psum_scatter(jnp.dot(attention, out_proj, preferred_element_type=jnp....]
    all_to_all x1 -> x0, blocking collectives: 42.3 us -> none  [on_device(): lax.all_to_all(own_table, 'sp', split_axis=0, concat_axis=0, tiled=True)]
    all_to_all x1 -> x0, waiting for transfers between devices: 36.5 us -> none  [on_device(): lax.all_to_all(routed_sum.astype(jnp.bfloat16), 'sp', split_axis=1, conca...]
    all_gather x1 -> x0, blocking collectives: 32.8 us -> none  [on_device(): rotary_piece = lax.all_gather(key_rot, 'sp', axis=0, tiled=True)]
    all_gather x3 -> x1, waiting for transfers between devices: 54.3 us -> 47.4 us  [on_device(): lax.all_gather(jnp.concatenate([latent_normed, key_rot], axis=1), 'sp', a...]
    reshape x1 -> x0, local copies, waits for them, and re-layouts: 6.25 us -> none  [on_device(): expert_out.reshape(column.shape).astype(jnp.float32).astype(jnp.bfloat16)]
  transfers between devices with their start and end apart: 7 -> 1, of which waited for: 5 -> 1; matrix products, arithmetic and copies ran while one was open for 12% -> 1% of each run, Pallas kernels for 0% -> 0%
where the time goes in v1:
time: 314 us; the launch traced here: 313 us
  Pallas kernels  175 us (56%)
  matrix products  52.1 us (17%)
  waiting for transfers between devices  47.4 us (15%)
  between operations  13.7 us (4%)
  local copies, waits for them, and re-layouts  12.5 us (4%)
  other arithmetic  11.9 us (4%)
    pallas_call x1, Pallas kernels, dispatch(): pl.pallas_call(functools.partial(dispatch_kernel, sp_count), out_shape=(j...  98.6 us
    pallas_call x1, Pallas kernels, give_back(): pl.pallas_call(functools.partial(return_kernel, sp_count), out_shape=(jax...  61.4 us
    all_gather x1, waiting for transfers between devices, on_device(): lax.all_gather(jnp.concatenate([latent_normed, key_rot], axis=1), 'sp', a...  47.4 us
    dot_general x2, matrix products, expert_block(): jnp.dot(hidden, down_part, preferred_element_type=jnp.float32)  18.4 us
    pallas_call x1, Pallas kernels, tp_reduce(): pl.pallas_call(reduce_kernel, out_shape=jax.ShapeDtypeStruct(parts.shape[...  15.4 us
    dot_general x2, matrix products, expert_block(): jnp.dot(expert_in, gate_part, preferred_element_type=jnp.float32)  7.4 us
    dot_general x1, matrix products, on_device(): jnp.dot(attention, out_proj, preferred_element_type=jnp.float32)  6.38 us
  transfers between devices with their start and end apart: 1, of which 1 were waited for; matrix products, arithmetic and copies ran while one was open for 1% of the time, Pallas kernels for 0%

profile of v1, /device:TPU:0, one launch (start us, length us, event | category | flops | bytes accessed | tf_op | source)
XLA Modules:
  0.0 313.1 jit_solution(12629257721316662597)
XLA Ops:
  14.1 47.4 %all-gather.2.cloned.1.call-done = bf16[1536,544]{1,0:T(8,128)(2,1)} async-done(((bf16[192,544]{1,0:T(8,128)(2,1)}), bf16[1536,544]{1,0:T(8,128)(2,1)}) %all-gather.2.cloned.1.call-update) | async-done | bytes 1671184 | tf_op jit(solution)/shard_map/all_gather | solution.py:474
  63.3 2.7 slice.34
  67.1 22.2 %while.18 = (s32[]{:T(128)}, f32[16,192]{1,0:T(8,128)S(1)}, f32[16,192]{1,0:T(8,128)S(1)}, f32[16,192,64]{1,2,0:T(8,128)}, s32[]{:T(128)}, /*index=5*/bf16[1536,...) while((s32[]{:T(128)}, f32[16,192]{1,0:T(8,128)S(1)}, ...), condition=%wide.region_6.7_spmd.clone, body=%wide.region_1.6_spmd.clone.sunk | while | flops 1591188224 | bytes 74948008 | solution.py:493
  67.1 22.1 %conditional.3 = ((f32[16,192]{1,0:T(8,128)S(1)}, f32[16,192]{1,0:T(8,128)S(1)}, f32[16,192,64]{1,2,0:T(8,128)})) conditional(s32[]{:T(128)} %convert_element_type.182, (f32[16,192]{1,0:T(8,128)S(1)}, f32[16,192]{1,0:T(8,128)S(1)}, f32[16,192,64]{1,2,0:T(8,128)}) %tuple.65, (s32[]{:T(128)}, s32[]{:T(128)}, bf16[1536,512]{1,0:T(8,128)(2,1)}, ...), branch_computations={%region_2.0_spmd, %region_3.5_spmd} | conditional | flops 1591188224 | bytes 74946960 | solution.py:486
  67.1 3.1 convolution_convert_fusion.1
  70.2 1.5 copy.65
  71.7 2.1 fusion.68
  74.0 2.9 fusion.67
  76.8 1.6 fusion.5
  79.5 2.8 convolution_convert_fusion
  82.3 1.5 copy.66
  83.8 5.4 %fusion.9 = f32[16,192,64]{1,2,0:T(8,128)} fusion(bf16[512,16,64]{0,2,1:T(8,128)(2,1)S(1)} %bitcast.81, f32[16,192,512]{2,1,0:T(8,128)} %copy-done.1, f32[16,192]{1,0:T(8,128)S(1)} %max.5, f32[16,192,64]{1,2,0:T(8,128)} %get-tuple-element.325, f32[16,192]{1,0:T(8,128)S(1)} %get-tuple-element.473), kind=kOutput, calls=%fused_computation.11 | convolution fusion | flops 204865536 | bytes 8937472 | tf_op jit(solution)/shard_map/while/body/eval_jaxpr/cond/branch_1_fun/hqk,khd->hqd/dot_general | solution.py:461
  89.3 1.3 divide_convert_fusion
  90.6 6.4 %convolution_convert_fusion.5 = bf16[192,4096]{1,0:T(8,128)(2,1)} fusion(bf16[192,1024]{0,1:T(8,128)(2,1)S(1)} %bitcast.90, bf16[1024,4096]{1,0:T(8,128)(2,1)} %param.31), kind=kOutput, calls=%fused_computation.27 | convolution fusion | flops 1611399168 | bytes 10354688 | tf_op jit(solution)/shard_map/dot_general | solution.py:504
  97.0 15.4 %shard_map.190 = f32[3,16,4096]{2,1,0:T(8,128)} custom-call(bf16[2,2,3,16,4096]{4,3,2,1,0:T(8,128)(2,1)} %bitcast.86), custom_call_target="tpu_custom_call" | custom-call | tf_op jit(solution)/shard_map/pallas_call | solution.py:195
  113.8 1.5 fusion.33
  115.5 1.8 convolution_convert_fusion.4
  117.3 98.6 %shard_map.191 = (bf16[4,8,24,4096]{3,2,1,0:T(8,128)(2,1)}, bf16[4,48,4096]{2,1,0:T(8,128)(2,1)}) custom-call(bf16[8,24,4096]{2,1,0:T(8,128)(2,1)} %bitcast.89, bf16[48,4096]{1,0:T(8,128)(2,1)} %copy-done.2), custom_call_target="tpu_custom_call" | custom-call | tf_op jit(solution)/shard_map/pallas_call | solution.py:296
  215.9 2.8 fusion.69
  218.7 4.6 %fusion.22 = f32[768,256]{1,0:T(8,128)S(1)} fusion(bf16[768,4096]{1,0:T(8,128)(2,1)} %bitcast.93, bf16[1,4096,256]{2,1,0:T(8,128)(2,1)S(1)} %copy-done.11), kind=kOutput, calls=%fused_computation.31 | convolution fusion | flops 1610612736 | bytes 9175040 | tf_op jit(solution)/shard_map/dot_general | solution.py:49
  223.3 5.7 %convolution_convert_fusion.3 = bf16[192,4096]{1,0:T(8,128)(2,1)} fusion(bf16[256,4096]{1,0:T(8,128)(2,1)} %param.42, bf16[192,4096]{1,0:T(8,128)(2,1)} %bitcast.85, bf16[4096,256]{1,0:T(8,128)(2,1)} %param.41, f32[192,256]{1,0:T(8,128)S(1)} %fusion.69), kind=kOutput, calls=%fused_computation.25 | convolution fusion | flops 806387712 | bytes 7536640 | tf_op jit(solution)/shard_map/dot_general | solution.py:52
  229.1 12.6 %convolution_convert_fusion.2 = bf16[768,4096]{1,0:T(8,128)(2,1)} fusion(bf16[1,256,4096]{2,1,0:T(8,128)(2,1)S(1)} %copy-done, bf16[768,4096]{1,0:T(8,128)(2,1)} %bitcast.94, bf16[1,4096,256]{2,1,0:T(8,128)(2,1)} %param.38, f32[768,256]{1,0:T(8,128)S(1)} %fusion.22), kind=kOutput, calls=%fused_computation.24 | convolution fusion | flops 3225550848 | bytes 17563648 | tf_op jit(solution)/shard_map/dot_general | solution.py:52
  241.7 61.4 %shard_map.192 = (bf16[8,24,4096]{2,1,0:T(8,128)(2,1)}, f32[3,16,4096]{2,1,0:T(8,128)}) custom-call(bf16[2,2,8,24,4096]{4,3,2,1,0:T(8,128)(2,1)} %bitcast.87, bf16[2,2,3,16,4096]{4,3,2,1,0:T(8,128)(2,1)} %bitcast.88), custom_call_target="tpu_custom_call" | custom-call | tf_op jit(solution)/shard_map/pallas_call | solution.py:366
  303.1 1.8 fusion.57
  (77 shorter events, 14.3 us)
Async XLA Ops:
  6.5 222.6 %copy-start = (bf16[1,256,4096]{2,1,0:T(8,128)(2,1)S(1)}, bf16[1,256,4096]{2,1,0:T(8,128)(2,1)}, u32[]{:S(2)}) copy-start(bf16[1,256,4096]{2,1,0:T(8,128)(2,1)} %param.39) | copy-start | bytes 6291460
  6.5 5.3 %copy-start.4 = (bf16[192,1024]{1,0:T(8,128)(2,1)S(1)}, bf16[192,1024]{1,0:T(8,128)(2,1)}, u32[]{:S(2)}) copy-start(bf16[192,1024]{1,0:T(8,128)(2,1)} %param.24) | copy-start | bytes 1179652
  6.5 6.3 %copy-start.9 = (s32[48,2]{0,1:T(2,128)S(1)}, s32[48,2]{0,1:T(2,128)}, u32[]{:S(2)}) copy-start(s32[48,2]{0,1:T(2,128)} %param.35) | copy-start | bytes 1156
  6.5 7.3 %copy-start.10 = (f32[48,2]{0,1:T(2,128)S(1)}, f32[48,2]{0,1:T(2,128)}, u32[]{:S(2)}) copy-start(f32[48,2]{0,1:T(2,128)} %param.36) | copy-start | bytes 1156
  6.5 54.9 %all-gather.2.cloned.1.call-start = ((), (), s32[]{:S(2)}) async-start(), calls=%async_computation | async-start | bytes 2211840 | tf_op jit(solution)/shard_map/all_gather | solution.py:474
  76.8 2.7 copy-start.1
  76.8 2.7 copy-start.12
  97.0 16.8 %copy-start.5 = (bf16[48,4096]{1,0:T(8,128)(2,1)S(1)}, bf16[48,4096]{1,0:T(8,128)(2,1)}, u32[]{:S(2)}) copy-start(bf16[48,4096]{1,0:T(8,128)(2,1)} %param.32) | copy-start | bytes 1179652
  97.0 16.8 %copy-start.6 = (f32[4096]{0:T(1024)S(1)}, f32[4096]{0:T(1024)}, u32[]{:S(2)}) copy-start(f32[4096]{0:T(1024)} %param.33) | copy-start | bytes 49156
  97.0 18.3 %copy-start.8 = (f32[4096]{0:T(1024)S(1)}, f32[4096]{0:T(1024)}, u32[]{:S(2)}) copy-start(f32[4096]{0:T(1024)} %param.34) | copy-start | bytes 49156
  115.5 1.9 copy-start.2
  215.9 2.8 copy-start.11
  303.1 1.9 copy-start.3
  303.1 2.1 copy-start.7
Sparse Core Ops, SparseCore 0:
  10.9 50.4 all-gather.1

commit v2 on v1

--- a/solution.py
+++ b/solution.py
@@ -379,6 +379,193 @@
         ],
         compiler_params=comm_params(2),
     )(parts, shared)
+
+
+def gather_kernel(sp_count, block, column, to_sp, to_low, to_high, relay):
+    me, tp_me = lax.axis_index("sp"), lax.axis_index("tp")
+    low_peer, high_peer = flip(tp_me, 1), flip(tp_me, 2)
+    last = sp_count - 1
+    enter(me, tp_me, sp_count)
+
+    def source_of(k):
+        return lax.rem(me + 2 * sp_count - 1 - k, sp_count)
+
+    def spread(k):
+        e = lax.rem(me + 1 + k, sp_count)
+        return remote_copy(
+            block, column.at[me, tp_me], to_sp.at[0, k], to_sp.at[1, k], e, tp_me
+        )
+
+    def forward(sems, k, source, slot, peer):
+        return remote_copy(
+            source, column.at[source_of(k), slot], sems.at[0, k], sems.at[1, k], me, peer
+        )
+
+    def own_low():
+        return forward(to_low, last, block, tp_me, low_peer)
+
+    def own_high():
+        return forward(to_high, last, block, tp_me, high_peer)
+
+    def low(k):
+        return forward(to_low, k, column.at[source_of(k), tp_me], tp_me, low_peer)
+
+    def high(k):
+        return forward(to_high, k, column.at[source_of(k), tp_me], tp_me, high_peer)
+
+    def relayed(k):
+        return forward(relay, k, column.at[source_of(k), high_peer], high_peer, low_peer)
+
+    loop(last, lambda k: spread(k).start())
+    own_high().start()
+    own_low().start()
+    column[me, tp_me] = block[...]
+
+    def arrive(k):
+        spread(k).wait_recv()
+        high(k).start()
+        low(k).start()
+
+    loop(last, arrive)
+
+    def pass_on(k):
+        high(k).wait_recv()
+        relayed(k).start()
+
+    pass_on(last)
+    loop(last, pass_on)
+
+    def settle(k):
+        low(k).wait_recv()
+        relayed(k).wait_recv()
+        relayed(k).wait_send()
+
+    loop(sp_count, settle)
+
+    def sent(k):
+        spread(k).wait_send()
+        low(k).wait_send()
+        high(k).wait_send()
+
+    loop(last, sent)
+    own_low().wait_send()
+    own_high().wait_send()
+
+
+def gather_blocks(block):
+    sp_count, tp_count = lax.axis_size("sp"), lax.axis_size("tp")
+    ring = pltpu.SemaphoreType.DMA((2, sp_count))
+    return pl.pallas_call(
+        functools.partial(gather_kernel, sp_count),
+        out_shape=jax.ShapeDtypeStruct((sp_count, tp_count) + block.shape, block.dtype),
+        in_specs=[IN_VMEM],
+        out_specs=IN_VMEM,
+        scratch_shapes=[ring, ring, ring, ring],
+        compiler_params=comm_params(3),
+    )(block)
+
+
+LANES = 128
+
+
+def attention_kernel(
+    chunk, scale, me, query, latents, key_up, value_up, out, keys, values, top, total, summed
+):
+    rows, pairs = query.shape[0], summed.shape[0]
+    latent_dim = value_up.shape[0]
+    first_query = me[0] * rows
+    top[...] = jnp.full_like(top, -1e30)
+    total[...] = jnp.zeros_like(total)
+    summed[...] = jnp.zeros_like(summed)
+    left_half = lax.broadcasted_iota(jnp.int32, (rows, LANES), 1) < VALUE_DIM
+    wide = 4 * LANES
+
+    def one_chunk(j, carry):
+        offset = pl.multiple_of(j * chunk, chunk)
+
+        def key_columns(n, inner):
+            columns = pl.ds(pl.multiple_of(n * wide, wide), wide)
+            keys[:, columns] = jnp.dot(
+                latents[pl.ds(offset, chunk), :],
+                key_up[:, columns],
+                preferred_element_type=jnp.float32,
+            ).astype(jnp.bfloat16)
+            return inner
+
+        def value_columns(n, inner):
+            columns = pl.ds(pl.multiple_of(n * wide, wide), wide)
+            values[:, columns] = jnp.dot(
+                latents[pl.ds(offset, chunk), :latent_dim],
+                value_up[:, columns],
+                preferred_element_type=jnp.float32,
+            ).astype(jnp.bfloat16)
+            return inner
+
+        lax.fori_loop(0, keys.shape[1] // wide, key_columns, 0)
+        lax.fori_loop(0, values.shape[1] // wide, value_columns, 0)
+
+        def one_pair(p, inner):
+            allowed = (
+                offset + lax.broadcasted_iota(jnp.int32, (rows, chunk), 1)
+            ) <= first_query + lax.broadcasted_iota(jnp.int32, (rows, chunk), 0)
+            pair_values = values[:, pl.ds(pl.multiple_of(p * LANES, LANES), LANES)]
+            factors, products = [], []
+            for half in range(2):
+                head = 2 * p + half
+                columns = pl.ds(pl.multiple_of(head * LANES, LANES), LANES)
+                scores = lax.dot_general(
+                    query[:, columns],
+                    keys[:, columns],
+                    (((1,), (1,)), ((), ())),
+                    preferred_element_type=jnp.float32,
+                )
+                scores = jnp.where(allowed, scores * scale, -1e30)
+                before = top[head]
+                newest = jnp.maximum(before, jnp.max(scores, axis=1, keepdims=True))
+                factor = jnp.exp(before - newest)
+                exponent = jnp.exp(scores - newest)
+                top[head] = newest
+                total[head] = total[head] * factor + jnp.sum(exponent, axis=1, keepdims=True)
+                factors.append(factor)
+                products.append(
+                    jnp.dot(
+                        exponent.astype(jnp.bfloat16),
+                        pair_values,
+                        preferred_element_type=jnp.float32,
+                    )
+                )
+            summed[p] = summed[p] * jnp.where(left_half, factors[0], factors[1]) + jnp.where(
+                left_half, products[0], products[1]
+            )
+            return inner
+
+        lax.fori_loop(0, pairs, one_pair, 0)
+        return carry
+
+    lax.fori_loop(0, (first_query + rows - 1) // chunk + 1, one_chunk, 0)
+    for p in range(pairs):
+        divisor = jnp.where(left_half, total[2 * p], total[2 * p + 1])
+        out[:, p * LANES : (p + 1) * LANES] = (summed[p] / divisor).astype(out.dtype)
+
+
+def attend_all(query, latents, key_up, value_up, scale):
+    rows = query.shape[0]
+    heads = query.shape[1] // LANES
+    chunk = math.gcd(latents.shape[0], 512)
+    return pl.pallas_call(
+        functools.partial(attention_kernel, chunk, scale),
+        out_shape=jax.ShapeDtypeStruct((rows, value_up.shape[1]), jnp.bfloat16),
+        in_specs=[pl.BlockSpec(memory_space=pltpu.SMEM)] + [IN_VMEM] * 4,
+        out_specs=IN_VMEM,
+        scratch_shapes=[
+            pltpu.VMEM((chunk, key_up.shape[1]), jnp.bfloat16),
+            pltpu.VMEM((chunk, value_up.shape[1]), jnp.bfloat16),
+            pltpu.VMEM((heads, rows, 1), jnp.float32),
+            pltpu.VMEM((heads, rows, 1), jnp.float32),
+            pltpu.VMEM((heads // 2, rows, LANES), jnp.float32),
+        ],
+        compiler_params=pltpu.CompilerParams(vmem_limit_bytes=60 * 1024 * 1024),
+    )(lax.axis_index("sp").astype(jnp.int32).reshape(1), query, latents, key_up, value_up)
 
 
 def dispatch_table(normed_rows, route_rows, route_weights, experts, capacity):
@@ -426,77 +613,48 @@
     local_rows = query_nope.shape[0]
     heads_here = query_nope.shape[1] // NOPE_DIM
     query_pos = lax.axis_index("sp") * local_rows + jnp.arange(local_rows, dtype=jnp.int32)
-    last_query = lax.axis_index("sp") * local_rows + local_rows - 1
     query_rot = rotate(
         query_rope.astype(jnp.float32).reshape(local_rows, heads_here, ROPE_DIM), query_pos[:, None]
     ).astype(jnp.bfloat16)
-    key_rot = rotate(key_rope.astype(jnp.float32), query_pos).astype(jnp.bfloat16)
-    latent_normed = rms_scale(latent.astype(jnp.float32), latent_gain).astype(jnp.bfloat16)
-    query_heads = query_nope.reshape(local_rows, heads_here, NOPE_DIM)
     score_scale = (NOPE_DIM + ROPE_DIM) ** (-0.5)
-
-    def attend(state_now, latent_rows, rotary_rows, key_start):
-        piece_rows = latent_rows.shape[0]
-        keys_here = jnp.dot(latent_rows, key_up, preferred_element_type=jnp.float32).astype(
-            jnp.bfloat16
-        )
-        keys_here = keys_here.reshape(piece_rows, heads_here, NOPE_DIM)
-        values_here = jnp.dot(latent_rows, value_up, preferred_element_type=jnp.float32).astype(
-            jnp.bfloat16
-        )
-        values_here = values_here.reshape(piece_rows, heads_here, VALUE_DIM)
-        scores = (
-            jnp.einsum("qhd,khd->hqk", query_heads, keys_here, preferred_element_type=jnp.float32)
-            + jnp.einsum("qhr,kr->hqk", query_rot, rotary_rows, preferred_element_type=jnp.float32)
-        ) * score_scale
-        allowed = (key_start + jnp.arange(piece_rows, dtype=jnp.int32))[None, :] <= query_pos[
-            :, None
-        ]
-        scores = jnp.where(allowed[None], scores, -1e30)
-        running, total_sum, summed = state_now
-        newest = jnp.maximum(running, jnp.max(scores, axis=-1))
-        factor = jnp.exp(running - newest)
-        exponent = jnp.exp(scores - newest[..., None])
-        total_sum = total_sum * factor + jnp.sum(exponent, axis=-1)
-        summed = summed * factor[..., None] + jnp.einsum(
-            "hqk,khd->hqd",
-            exponent.astype(jnp.bfloat16),
-            values_here,
-            preferred_element_type=jnp.float32,
-        )
-        return (newest, total_sum, summed)
-
-    initial = (
-        jnp.full((heads_here, local_rows), -1e30, jnp.float32),
-        jnp.zeros((heads_here, local_rows), jnp.float32),
-        jnp.zeros((heads_here, local_rows, VALUE_DIM), jnp.float32),
-    )
-    gathered = lax.all_gather(
-        jnp.concatenate([latent_normed, key_rot], axis=1), "sp", axis=0, tiled=True
-    )
-    latent_piece = gathered[:, : latent.shape[1]]
-    rotary_piece = gathered[:, latent.shape[1] :]
-    piece_rows = latent_piece.shape[0]
-    step_rows = math.gcd(piece_rows, 512)
-
-    def one_step(step_index, inner_state):
-        offset = step_index * step_rows
-        latent_rows = lax.dynamic_slice_in_dim(latent_piece, offset, step_rows, 0)
-        rotary_rows = lax.dynamic_slice_in_dim(rotary_piece, offset, step_rows, 0)
-        return lax.cond(
-            offset <= last_query,
-            lambda carried: attend(carried, latent_rows, rotary_rows, offset),
-            lambda carried: carried,
-            inner_state,
-        )
-
-    running, total_sum, summed = lax.fori_loop(0, piece_rows // step_rows, one_step, initial)
-    attention = (
-        (summed / total_sum[..., None])
-        .transpose(1, 0, 2)
-        .reshape(local_rows, heads_here * VALUE_DIM)
-    )
-    attention = attention.astype(jnp.bfloat16)
+    latent_dim = latent.shape[1]
+    spare = LANES - NOPE_DIM - ROPE_DIM
+    share = local_rows // lax.axis_size("tp")
+    start = lax.axis_index("tp") * share
+    share_pos = lax.axis_index("sp") * local_rows + start + jnp.arange(share, dtype=jnp.int32)
+    latent_share = lax.dynamic_slice_in_dim(latent, start, share, 0)
+    rope_share = lax.dynamic_slice_in_dim(key_rope, start, share, 0)
+    block = jnp.concatenate(
+        [
+            rms_scale(latent_share.astype(jnp.float32), latent_gain).astype(jnp.bfloat16),
+            rotate(rope_share.astype(jnp.float32), share_pos).astype(jnp.bfloat16),
+            jnp.zeros((share, LANES - ROPE_DIM), jnp.bfloat16),
+        ],
+        axis=1,
+    )
+    latents = gather_blocks(block).reshape(-1, latent_dim + LANES)
+    query = jnp.concatenate(
+        [
+            query_nope.reshape(local_rows, heads_here, NOPE_DIM),
+            query_rot,
+            jnp.zeros((local_rows, heads_here, spare), jnp.bfloat16),
+        ],
+        axis=2,
+    ).reshape(local_rows, heads_here * LANES)
+    pass_rotary = jnp.eye(LANES, LANES, NOPE_DIM, dtype=jnp.bfloat16) * (
+        jnp.arange(LANES) < ROPE_DIM
+    ).astype(jnp.bfloat16)[:, None]
+    key_map = jnp.concatenate(
+        [
+            jnp.pad(
+                key_up.reshape(latent_dim, heads_here, NOPE_DIM),
+                ((0, 0), (0, 0), (0, LANES - NOPE_DIM)),
+            ).reshape(latent_dim, heads_here * LANES),
+            jnp.tile(pass_rotary, (1, heads_here)),
+        ],
+        axis=0,
+    )
+    attention = attend_all(query, latents, key_map, value_up, score_scale)
     rows_here = resid.shape[0]
     model_dim = resid.shape[1]
     piece = math.gcd(rows_here, 16)

time: 314 us -> 258 us (0.82)
  waiting for transfers between devices: 47.4 us -> 0 us
  Pallas kernels: 175 us -> 195 us
  matrix products: 52.1 us -> 37.4 us
  between operations: 13.7 us -> 0.32 us
    all_gather x1 -> x0, waiting for transfers between devices: 47.4 us -> none  [on_device(): lax.all_gather(jnp.concatenate([latent_normed, key_rot], axis=1), 'sp', a...]
    pallas_call x0 -> x2, Pallas kernels: none -> 40.9 us  [the longest x1 25.6 us: gather_blocks(): pl.pallas_call(functools.partial(gather_kernel, sp_count), out_shape=jax....]
    pallas_call x1, Pallas kernels: 98.6 us -> 76.6 us  [dispatch(): pl.pallas_call(functools.partial(dispatch_kernel, sp_count), out_shape=(j...]
    dot_general x5 -> x0, matrix products: 16.2 us -> none  [the longest x1 5.43 us: attend(): jnp.einsum('hqk,khd->hqd', exponent.astype(jnp.bfloat16), values_here, pr...]
    concatenate x2 -> x3, other arithmetic: 0.82 us -> 5.49 us  [the longest x1 3.41 us: on_device(): jnp.concatenate([jnp.pad(key_up.reshape(latent_dim, heads_here, NOPE_DIM)...]
    reshape x1 -> x2, local copies, waits for them, and re-layouts: 1.06 us -> 5.19 us  [the longest x1 3.95 us: on_device(): key_map = jnp.concatenate([jnp.pad(key_up.reshape(latent_dim, heads_here,...]
    slice x2 -> x0, local copies, waits for them, and re-layouts: 3.67 us -> none  [the longest x1 2.65 us: on_device(): latent_piece = gathered[:, :latent.shape[1]]]
  transfers between devices with their start and end apart: 1 -> 0, of which waited for: 1 -> 0; matrix products, arithmetic and copies ran while one was open for 1% -> 0% of each run, Pallas kernels for 0% -> 0%
where the time goes in v2:
time: 258 us; the launch traced here: 257 us
  Pallas kernels  195 us (76%)
  matrix products  37.4 us (14%)
  other arithmetic  12.8 us (5%)
  local copies, waits for them, and re-layouts  11.2 us (4%)
    pallas_call x1, Pallas kernels, dispatch(): pl.pallas_call(functools.partial(dispatch_kernel, sp_count), out_shape=(j...  76.6 us
    pallas_call x1, Pallas kernels, give_back(): pl.pallas_call(functools.partial(return_kernel, sp_count), out_shape=(jax...  62.5 us
    pallas_call x1, Pallas kernels, gather_blocks(): pl.pallas_call(functools.partial(gather_kernel, sp_count), out_shape=jax....  25.6 us
    dot_general x2, matrix products, expert_block(): jnp.dot(hidden, down_part, preferred_element_type=jnp.float32)  18.5 us
    pallas_call x1, Pallas kernels, tp_reduce(): pl.pallas_call(reduce_kernel, out_shape=jax.ShapeDtypeStruct(parts.shape[...  15.4 us
    pallas_call x1, Pallas kernels, attend_all(): pl.pallas_call(functools.partial(attention_kernel, chunk, scale), out_sha...  15.3 us
    dot_general x2, matrix products, expert_block(): jnp.dot(expert_in, gate_part, preferred_element_type=jnp.float32)  8.72 us
    dot_general x1, matrix products, on_device(): jnp.dot(attention, out_proj, preferred_element_type=jnp.float32)  6.49 us

profile of v2, /device:TPU:0, one launch (start us, length us, event | category | flops | bytes accessed | tf_op | source)
XLA Modules:
  0.0 257.1 jit_solution(8187655234666928236)
XLA Ops:
  0.0 1.1 fusion.33
  1.1 0.9 fusion.35
  3.9 25.6 %shard_map.190 = bf16[8,4,48,640]{3,2,1,0:T(8,128)(2,1)} custom-call(bf16[48,640]{1,0:T(8,128)(2,1)} %maximum_maximum_fusion.1.block), custom_call_target="tpu_custom_call" | custom-call | tf_op jit(solution)/shard_map/pallas_call | solution.py:458
  29.9 1.0 copy.46
  31.0 1.4 maximum_maximum_fusion
  32.4 1.2 copy.55.query
  33.6 1.5 copy.51
  35.1 1.6 pad.4
  36.7 4.0 %copy.56 = bf16[512,2048]{1,0:T(8,128)(2,1)} copy(bf16[512,2048]{0,1:T(8,128)(2,1)} %bitcast.69) | data formatting | bytes 4194304 | tf_op jit(solution)/shard_map/reshape | solution.py:652
  41.0 3.4 %pad_maximum_fusion.key_up = bf16[640,2048]{1,0:T(8,128)(2,1)} fusion(bf16[128,2048]{1,0:T(8,128)(2,1)S(1)} %bitcast.76, bf16[512,2048]{1,0:T(8,128)(2,1)} %copy.56), kind=kLoop, calls=%fused_computation.4 | loop fusion | flops 5242880 | bytes 5242880 | tf_op jit(solution)/shard_map/concatenate | solution.py:647
  44.4 15.3 %shard_map.191 = bf16[192,1024]{1,0:T(8,128)(2,1)} custom-call(s32[1]{0:T(128)} %bitcast.me, bf16[192,2048]{1,0:T(8,128)(2,1)} %copy.55.query, bf16[1536,640]{1,0:T(8,128)(2,1)} %bitcast.70, bf16[640,2048]{1,0:T(8,128)(2,1)} %pad_maximum_fusion.key_up, bf16[512,1024]{1,0:T(8,128)(2,1)} %value_up.1), custom_call_target="tpu_custom_call" | custom-call | tf_op jit(solution)/shard_map/pallas_call | solution.py:555
  59.7 6.5 %convolution_convert_fusion.3 = bf16[192,4096]{1,0:T(8,128)(2,1)} fusion(bf16[192,1024]{1,0:T(8,128)(2,1)} %shard_map.191, bf16[1024,4096]{1,0:T(8,128)(2,1)} %param.27), kind=kOutput, calls=%fused_computation.3 | convolution fusion | flops 1611399168 | bytes 10354688 | tf_op jit(solution)/shard_map/dot_general | solution.py:662
  66.2 15.4 %shard_map.192 = f32[3,16,4096]{2,1,0:T(8,128)} custom-call(bf16[2,2,3,16,4096]{4,3,2,1,0:T(8,128)(2,1)} %bitcast.80), custom_call_target="tpu_custom_call" | custom-call | tf_op jit(solution)/shard_map/pallas_call | solution.py:195
  81.6 1.3 multiply_reduce_fusion.1
  83.0 1.5 fusion.14
  85.6 1.8 convolution_convert_fusion.2
  87.5 76.6 %shard_map.193 = (bf16[4,8,24,4096]{3,2,1,0:T(8,128)(2,1)}, bf16[4,48,4096]{2,1,0:T(8,128)(2,1)}) custom-call(bf16[8,24,4096]{2,1,0:T(8,128)(2,1)} %bitcast.73, bf16[48,4096]{1,0:T(8,128)(2,1)} %copy-done.1), custom_call_target="tpu_custom_call" | custom-call | tf_op jit(solution)/shard_map/pallas_call | solution.py:296
  164.1 2.6 %fusion.57 = f32[192,256]{1,0:T(8,128)S(1)} fusion(bf16[192,4096]{1,0:T(8,128)(2,1)} %bitcast.67, bf16[4096,256]{1,0:T(8,128)(2,1)} %param.36), kind=kOutput, calls=%fused_computation.92 | convolution fusion | flops 402653184 | bytes 3866624 | tf_op jit(solution)/shard_map/dot_general | solution.py:49
  166.8 5.7 %convolution_convert_fusion.1 = bf16[192,4096]{1,0:T(8,128)(2,1)} fusion(bf16[256,4096]{1,0:T(8,128)(2,1)} %param.38, bf16[192,4096]{1,0:T(8,128)(2,1)} %bitcast.68, bf16[4096,256]{1,0:T(8,128)(2,1)} %param.37, f32[192,256]{1,0:T(8,128)S(1)} %fusion.57), kind=kOutput, calls=%fused_computation.1 | convolution fusion | flops 806387712 | bytes 7536640 | tf_op jit(solution)/shard_map/dot_general | solution.py:52
  172.5 6.1 %fusion.3 = f32[768,256]{1,0:T(8,128)} fusion(bf16[768,4096]{1,0:T(8,128)(2,1)} %bitcast.82, bf16[1,4096,256]{2,1,0:T(8,128)(2,1)} %param.33), kind=kOutput, calls=%fused_computation.8 | convolution fusion | flops 1610612736 | bytes 9175040 | tf_op jit(solution)/shard_map/dot_general | solution.py:49
  178.6 12.8 %convolution_convert_fusion = bf16[768,4096]{1,0:T(8,128)(2,1)} fusion(bf16[1,256,4096]{2,1,0:T(8,128)(2,1)S(1)} %copy-done, bf16[768,4096]{1,0:T(8,128)(2,1)} %bitcast.83, bf16[1,4096,256]{2,1,0:T(8,128)(2,1)} %param.34, f32[768,256]{1,0:T(8,128)} %fusion.3), kind=kOutput, calls=%fused_computation | convolution fusion | flops 3225550848 | bytes 17563648 | tf_op jit(solution)/shard_map/dot_general | solution.py:52
  191.4 62.5 %shard_map.194 = (bf16[8,24,4096]{2,1,0:T(8,128)(2,1)}, f32[3,16,4096]{2,1,0:T(8,128)}) custom-call(bf16[2,2,8,24,4096]{4,3,2,1,0:T(8,128)(2,1)} %bitcast.71, bf16[2,2,3,16,4096]{4,3,2,1,0:T(8,128)(2,1)} %bitcast.72), custom_call_target="tpu_custom_call" | custom-call | tf_op jit(solution)/shard_map/pallas_call | solution.py:366
  254.0 1.9 fusion.39
  256.1 1.0 fusion.17
  (61 shorter events, 4.2 us)
Async XLA Ops:
  0.0 178.6 %copy-start = (bf16[1,256,4096]{2,1,0:T(8,128)(2,1)S(1)}, bf16[1,256,4096]{2,1,0:T(8,128)(2,1)}, u32[]{:S(2)}) copy-start(bf16[1,256,4096]{2,1,0:T(8,128)(2,1)} %param.35) | copy-start | bytes 6291460
  0.0 29.6 %copy-start.5 = (bf16[192,512]{1,0:T(8,128)(2,1)S(1)}, bf16[192,512]{1,0:T(8,128)(2,1)}, u32[]{:S(2)}) copy-start(bf16[192,512]{1,0:T(8,128)(2,1)} %param.21) | copy-start | bytes 589828
  3.9 26.0 %copy-start.3 = (bf16[192,1024]{1,0:T(8,128)(2,1)S(1)}, bf16[192,1024]{1,0:T(8,128)(2,1)}, u32[]{:S(2)}) copy-start(bf16[192,1024]{1,0:T(8,128)(2,1)} %param.20) | copy-start | bytes 1179652
  66.2 16.8 %copy-start.4 = (bf16[48,4096]{1,0:T(8,128)(2,1)S(1)}, bf16[48,4096]{1,0:T(8,128)(2,1)}, u32[]{:S(2)}) copy-start(bf16[48,4096]{1,0:T(8,128)(2,1)} %param.28) | copy-start | bytes 1179652
  66.2 16.8 %copy-start.6 = (f32[4096]{0:T(1024)S(1)}, f32[4096]{0:T(1024)}, u32[]{:S(2)}) copy-start(f32[4096]{0:T(1024)} %param.29) | copy-start | bytes 49156
  66.2 18.3 %copy-start.8 = (f32[4096]{0:T(1024)S(1)}, f32[4096]{0:T(1024)}, u32[]{:S(2)}) copy-start(f32[4096]{0:T(1024)} %param.30) | copy-start | bytes 49156
  81.6 3.1 %copy-start.9 = (s32[48,2]{0,1:T(2,128)S(1)}, s32[48,2]{0,1:T(2,128)}, u32[]{:S(2)}) copy-start(s32[48,2]{0,1:T(2,128)} %param.31) | copy-start | bytes 1156
  84.7 2.8 %copy-start.1 = (bf16[48,4096]{1,0:T(8,128)(2,1)}, bf16[48,4096]{1,0:T(8,128)(2,1)S(1)}, u32[]{:S(2)}) copy-start(bf16[48,4096]{1,0:T(8,128)(2,1)S(1)} %fusion.16.normed) | copy-start | bytes 1179652
  191.4 62.5 %copy-start.10 = (f32[48,2]{0,1:T(2,128)S(1)}, f32[48,2]{0,1:T(2,128)}, u32[]{:S(2)}) copy-start(f32[48,2]{0,1:T(2,128)} %param.32) | copy-start | bytes 1156
  253.9 2.0 copy-start.2
  254.0 2.1 copy-start.7
